TPU v7x, 32 devices: a whole 2x2x4 slice. The times are simulated.
32 devices in a mesh: ep: 8 (over z, y), tp: 4 (over x, core).
Axes of the slice: x: 2, y: 2, z: 4, core: 2. Of those that a mesh axis runs over, the one named last changes fastest.
Arguments:
- tokens: bfloat16 [1344, 2048], P('ep'), may hold values from -6 to 6
- cotangent: bfloat16 [1344, 2048], P('ep'), may hold values from -6 to 6
- group_ids: int32 [1344, 1], P('ep'), may hold values from 0 to 7; in each aligned block of 168 rows (0 to 167, 168 to 335, ...) at most 32 rows name the same one
- within_ids: int32 [1344, 2], P('ep'), may hold values from 0 to 1, all different within a row
- gate_weights: bfloat16 [1344, 2], P('ep'), may hold values from 0.099609375 to 1
- w_gate: bfloat16 [16, 2048, 1024], P('ep', None, 'tp'), may hold values from -0.125 to 0.125
- w_up: bfloat16 [16, 2048, 1024], P('ep', None, 'tp'), may hold values from -0.125 to 0.125
- w_down: bfloat16 [16, 1024, 2048], P('ep', 'tp'), may hold values from -0.1875 to 0.1875
Outputs:
- tokens_grad: bfloat16 [1344, 2048], P('ep', 'tp')
- gate_grad: float32 [1344, 2], P('ep')
- w_gate_grad: bfloat16 [16, 2048, 1024], P('ep', None, 'tp')
- w_up_grad: bfloat16 [16, 2048, 1024], P('ep', None, 'tp')
- w_down_grad: bfloat16 [16, 1024, 2048], P('ep', 'tp')
Inputs may be any that keep to these rules, and one draw needn't show every extreme that they name: `group_ids`: in the rows of one device no group is chosen by more than 32 rows. `within_ids`: the two entries of a row differ.
All inputs are finite; a program needn't handle non-finite values.
Results may differ from a plain program's by a relative error of at most 0.017.
Values may be sent and summed in bfloat16 or wider, within the bound.
A program may use at most 64 MiB of HBM per device.

v0:
```python
import jax
import jax.numpy as jnp
from jax import lax
from jax.sharding import PartitionSpec as P


def on_device(tokens, cotangent, group_ids, within_ids, gate_weights, w_gate, w_up, w_down):
    ep_count = lax.axis_size("ep")
    tp_count = lax.axis_size("tp")
    tok_rows, feat_width = tokens.shape
    experts_here = w_gate.shape[0]
    capacity = (3 * tok_rows + 2 * ep_count - 1) // (2 * ep_count)
    slot_count = ep_count * capacity
    group_of = group_ids[:, 0]
    in_group = (group_of[:, None] == jnp.arange(ep_count, dtype=jnp.int32)[None, :]).astype(
        jnp.float32
    )
    row_index = jnp.arange(tok_rows, dtype=jnp.int32)
    tri_lower = (row_index[:, None] > row_index[None, :]).astype(jnp.float32)
    before = jnp.dot(tri_lower, in_group, precision=lax.Precision.HIGHEST)
    rank_in = jnp.sum(before * in_group, axis=1).astype(jnp.int32)
    target = group_of * capacity + rank_in
    placing = jnp.arange(slot_count, dtype=jnp.int32)[:, None] == target[None, :]
    place_b = placing.astype(jnp.bfloat16)
    local_ids = jnp.arange(experts_here, dtype=jnp.int32)
    chosen = (within_ids[:, :, None] == local_ids[None, None, :]).astype(jnp.float32)
    combine = jnp.sum(chosen * gate_weights.astype(jnp.float32)[:, :, None], axis=1).astype(
        jnp.bfloat16
    )

    def arrange(source):
        placed = jnp.dot(place_b, source, preferred_element_type=jnp.float32).astype(jnp.bfloat16)
        return placed.reshape(ep_count, capacity, source.shape[1])

    col_share = feat_width // tp_count
    col_start = lax.axis_index("tp") * col_share
    part_x = lax.dynamic_slice_in_dim(tokens, col_start, col_share, 1)
    part_dy = lax.dynamic_slice_in_dim(cotangent, col_start, col_share, 1)
    thin_x, thin_dy, moved_comb = (
        lax.all_to_all(arrange(part_x), "ep", split_axis=0, concat_axis=0, tiled=True),
        lax.all_to_all(arrange(part_dy), "ep", split_axis=0, concat_axis=0, tiled=True),
        lax.all_to_all(arrange(combine), "ep", split_axis=0, concat_axis=0, tiled=True),
    )
    moved_x, moved_dy = (
        lax.all_gather(thin_x, "tp", axis=2, tiled=True),
        lax.all_gather(thin_dy, "tp", axis=2, tiled=True),
    )
    slot_x = moved_x.reshape(slot_count, feat_width)
    slot_dy = moved_dy.reshape(slot_count, feat_width)
    slot_comb = moved_comb.reshape(slot_count, experts_here)
    dy_float = slot_dy.astype(jnp.float32)
    dx_total = jnp.zeros((slot_count, feat_width), jnp.float32)
    gate_parts = []
    grads_gate = []
    grads_up = []
    grads_down = []
    for expert in range(experts_here):
        pre_gate = jnp.dot(slot_x, w_gate[expert], preferred_element_type=jnp.float32)
        pre_up = jnp.dot(slot_x, w_up[expert], preferred_element_type=jnp.float32)
        sig_gate = jax.nn.sigmoid(pre_gate)
        act_b = (pre_gate * sig_gate * pre_up).astype(jnp.bfloat16)
        down_part = jnp.dot(act_b, w_down[expert], preferred_element_type=jnp.float32)
        gate_parts.append(jnp.sum(dy_float * down_part, axis=1))
        scaled = (slot_comb[:, expert : expert + 1].astype(jnp.float32) * dy_float).astype(
            jnp.bfloat16
        )
        grads_down.append(
            jnp.einsum("sf,sd->fd", act_b, scaled, preferred_element_type=jnp.float32).astype(
                jnp.bfloat16
            )
        )
        act_grad = jnp.einsum(
            "sd,fd->sf", scaled, w_down[expert], preferred_element_type=jnp.float32
        )
        gate_b = (act_grad * pre_up * sig_gate * (1.0 + pre_gate * (1.0 - sig_gate))).astype(
            jnp.bfloat16
        )
        up_b = (act_grad * pre_gate * sig_gate).astype(jnp.bfloat16)
        grads_gate.append(
            jnp.einsum("sd,sf->df", slot_x, gate_b, preferred_element_type=jnp.float32).astype(
                jnp.bfloat16
            )
        )
        grads_up.append(
            jnp.einsum("sd,sf->df", slot_x, up_b, preferred_element_type=jnp.float32).astype(
                jnp.bfloat16
            )
        )
        dx_total = dx_total + jnp.einsum(
            "sf,df->sd", gate_b, w_gate[expert], preferred_element_type=jnp.float32
        )
        dx_total = dx_total + jnp.einsum(
            "sf,df->sd", up_b, w_up[expert], preferred_element_type=jnp.float32
        )
    gate_part = jnp.stack(gate_parts, axis=1)
    dx_share = lax.psum_scatter(
        dx_total.astype(jnp.bfloat16), "tp", scatter_dimension=1, tiled=True
    )
    gate_sum = lax.psum(gate_part, "tp")
    back_dx = lax.all_to_all(
        dx_share.reshape(ep_count, capacity, dx_share.shape[1]),
        "ep",
        split_axis=0,
        concat_axis=0,
        tiled=True,
    )
    back_gate = lax.all_to_all(
        gate_sum.reshape(ep_count, capacity, experts_here),
        "ep",
        split_axis=0,
        concat_axis=0,
        tiled=True,
    )
    tokens_grad = jnp.einsum(
        "st,sd->td",
        place_b,
        back_dx.reshape(slot_count, dx_share.shape[1]),
        preferred_element_type=jnp.float32,
    ).astype(jnp.bfloat16)
    dense_gate = jnp.einsum(
        "st,se->te",
        placing.astype(jnp.float32),
        back_gate.reshape(slot_count, experts_here),
        precision=lax.Precision.HIGHEST,
    )
    gate_grad = jnp.sum(chosen * dense_gate[:, None, :], axis=2)
    return (
        tokens_grad,
        gate_grad,
        jnp.stack(grads_gate),
        jnp.stack(grads_up),
        jnp.stack(grads_down),
    )


def solution(mesh):
    in_specs = (
        P("ep", None),
        P("ep", None),
        P("ep", None),
        P("ep", None),
        P("ep", None),
        P("ep", None, "tp"),
        P("ep", None, "tp"),
        P("ep", "tp", None),
    )
    out_specs = (
        P("ep", "tp"),
        P("ep", None),
        P("ep", None, "tp"),
        P("ep", None, "tp"),
        P("ep", "tp", None),
    )
    return jax.shard_map(
        on_device, mesh=mesh, in_specs=in_specs, out_specs=out_specs, check_vma=False
    )
```

profile of v0, /device:TPU:0, one launch (start us, length us, event | category | flops | bytes accessed | tf_op | source)
XLA Modules:
  0.0 144.7 jit_solution(13215352288851334555)
XLA Ops:
  7.2 0.0 copy-start
  7.2 0.0 all-gather.5.cloned.1.call-start
  7.2 0.9 fusion.11
  8.1 0.7 convert_add_fusion
  8.8 0.2 convolution_convert_fusion.6
  9.1 16.1 %all_to_all.25 = bf16[8,32,512]{2,1,0:T(8,128)(2,1)} all-to-all(bf16[8,32,512]{2,1,0:T(8,128)(2,1)S(1)} %bitcast.119), channel_id=1, replica_groups=mesh['ep'=8,'tp'=4] {'ep'}, dimensions={0} | all-to-all | bytes 524288 | tf_op jit(solution)/shard_map/all_to_all | solution.py:40
  25.2 0.0 all-gather.5.cloned.1.call-update
  25.2 0.0 all-gather.3.cloned.1.call-start
  25.3 1.1 convolution_convert_fusion.7
  26.4 12.1 %all_to_all.26 = bf16[8,32,512]{2,1,0:T(8,128)(2,1)} all-to-all(bf16[8,32,512]{2,1,0:T(8,128)(2,1)S(1)} %bitcast.118), channel_id=1, replica_groups=mesh['ep'=8,'tp'=4] {'ep'}, dimensions={0} | all-to-all | bytes 524288 | tf_op jit(solution)/shard_map/all_to_all | solution.py:41
  38.5 0.0 all-gather.3.cloned.1.call-update
  38.5 2.6 %all-gather.5.cloned.1.call-done = bf16[8,32,2048]{2,1,0:T(8,128)(2,1)} async-done(((bf16[8,32,512]{2,1,0:T(8,128)(2,1)}), bf16[8,32,2048]{2,1,0:T(8,128)(2,1)}) %all-gather.5.cloned.1.call-update) | async-done | bytes 1048592 | tf_op jit(solution)/shard_map/all_gather | solution.py:45
  41.1 2.1 %fusion.23 = f32[256,256]{1,0:T(8,128)S(1)} fusion(bf16[256,2048]{1,0:T(8,128)(2,1)} %bitcast.105, bf16[2,2048,256]{2,1,0:T(8,128)(2,1)} %param.13), kind=kOutput, calls=%fused_computation.46 | convolution fusion | flops 268435456 | bytes 2359296 | tf_op jit(solution)/shard_map/dot_general | solution.py:58
  43.2 1.7 %fusion.13 = f32[256,256]{1,0:T(8,128)S(1)} fusion(bf16[256,2048]{1,0:T(8,128)(2,1)S(1)} %bitcast.106, bf16[2,2048,256]{2,1,0:T(8,128)(2,1)} %param.13), kind=kOutput, calls=%fused_computation.36 | convolution fusion | flops 268435456 | bytes 2359296 | tf_op jit(solution)/shard_map/dot_general | solution.py:58
  44.9 0.0 copy-start.13
  44.9 1.1 multiply_convert_fusion.3
  46.1 1.1 multiply_convert_fusion.2
  47.2 12.2 %all-gather.3.cloned.1.call-done = bf16[8,32,2048]{2,1,0:T(8,128)(2,1)} async-done(((bf16[8,32,512]{2,1,0:T(8,128)(2,1)}), bf16[8,32,2048]{2,1,0:T(8,128)(2,1)}) %all-gather.3.cloned.1.call-update) | async-done | bytes 1048592 | tf_op jit(solution)/shard_map/all_gather | solution.py:46
  59.4 2.1 %fusion.10 = f32[256]{0:T(256)S(1)} fusion(bf16[256,256]{1,0:T(8,128)(2,1)S(1)} %get-tuple-element.19, bf16[2,256,2048]{2,1,0:T(8,128)(2,1)} %param.15, bf16[256,2048]{1,0:T(8,128)(2,1)} %bitcast.113), kind=kOutput, calls=%fused_computation.28 | convolution fusion | flops 270008064 | bytes 2229248 | tf_op jit(solution)/shard_map/dot_general | solution.py:62
  61.5 0.0 copy-start.10
  61.6 1.8 %fusion.9 = f32[256]{0:T(256)S(1)} fusion(bf16[256,256]{1,0:T(8,128)(2,1)S(1)} %get-tuple-element.21, bf16[2,256,2048]{2,1,0:T(8,128)(2,1)} %param.15, bf16[256,2048]{1,0:T(8,128)(2,1)S(1)} %bitcast.114), kind=kOutput, calls=%fused_computation.27 | convolution fusion | flops 270008064 | bytes 2229248 | tf_op jit(solution)/shard_map/dot_general | solution.py:62
  63.4 0.1 reshape.71
  63.4 6.5 %psum.7 = f32[8,32,2]{1,2,0:T(2,128)} all-reduce(f32[8,32,2]{1,2,0:T(2,128)S(1)} %copy.33), channel_id=1, replica_groups=mesh['ep'=8,'tp'=4] {'tp'}, use_global_device_ids=true, to_apply=%region_5.0 | all-reduce | flops 512 | bytes 4096 | tf_op jit(solution)/shard_map/psum | solution.py:99
  70.0 5.7 %all-to-all-start.4 = ((f32[8,32,2]{1,2,0:T(2,128)}), f32[8,32,2]{1,2,0:T(2,128)S(1)}, u32[]{:S(2)}, u32[]{:S(2)}) async-start(f32[8,32,2]{1,2,0:T(2,128)} %psum.7), calls=%async_computation.5 | async-start | bytes 16384 | tf_op jit(solution)/shard_map/all_to_all | solution.py:107
  75.7 0.0 reduce-scatter.2.cloned.1.call-start
  75.7 6.5 %all-to-all-done.4 = f32[8,32,2]{1,2,0:T(2,128)S(1)} async-done(((f32[8,32,2]{1,2,0:T(2,128)}), f32[8,32,2]{1,2,0:T(2,128)S(1)}, u32[]{:S(2)}, u32[]{:S(2)}) %all-to-all-start.4) | async-done | bytes 2080 | tf_op jit(solution)/shard_map/all_to_all | solution.py:107
  82.2 0.1 reshape.72
  82.3 0.2 fusion.43
  82.4 0.6 select_reduce_fusion
  83.1 0.2 convolution_convert_fusion.9
  83.2 0.1 reshape.64
  83.3 8.9 %all_to_all.27 = bf16[8,32,2]{1,2,0:T(2,128)(2,1)S(1)} all-to-all(bf16[8,32,2]{1,2,0:T(2,128)(2,1)S(1)} %copy.31), channel_id=1, replica_groups=mesh['ep'=8,'tp'=4] {'ep'}, dimensions={0} | all-to-all | bytes 2048 | tf_op jit(solution)/shard_map/all_to_all | solution.py:42
  92.2 0.1 reshape.65
  92.3 0.1 mul.135
  92.4 0.1 mul.125
  92.5 0.4 multiply_convert_fusion
  92.9 1.2 copy-done.12
  94.1 1.6 %multiply_convert_fusion.6 = (bf16[256,256]{1,0:T(8,128)(2,1)S(1)}, bf16[256,256]{1,0:T(8,128)(2,1)S(1)}) fusion(f32[256,256]{1,0:T(8,128)S(1)} %fusion.23, f32[256,256]{1,0:T(8,128)} %get-tuple-element.22, bf16[256,2048]{1,0:T(8,128)(2,1)S(1)} %bitcast.116, bf16[2,256,2048]{2,1,0:T(8,128)(2,1)S(1)} %copy-done.12), kind=kOutput, calls=%fused_computation.71 | convolution fusion | flops 269287424 | bytes 2883584 | tf_op jit(solution)/shard_map/sd,fd->sf/dot_general | solution.py:72
  95.7 0.1 copy-done.5
  95.8 0.5 fusion.21
  96.2 1.1 copy-done.7
  97.3 0.5 convolution_add_fusion.2
  97.8 0.5 copy-done.14
  98.2 0.1 copy-done.15
  98.3 0.5 multiply_convert_fusion.4
  98.8 0.5 convolution_add_fusion.1
  99.3 1.5 %fusion = bf16[256,2048]{1,0:T(8,128)(2,1)} fusion(f32[256,2048]{1,0:T(8,128)S(1)} %convolution_add_fusion.1, bf16[256,256]{1,0:T(8,128)(2,1)S(1)} %get-tuple-element.13, bf16[2,2048,256]{2,1,0:T(8,128)(2,1)S(1)} %copy-done.7), kind=kOutput, calls=%fused_computation.5 | convolution fusion | flops 269484032 | bytes 4325376 | tf_op jit(solution)/shard_map/sf,df->sd/dot_general | solution.py:92
  100.7 0.0 reduce-scatter.2.cloned.1.call-update
  100.8 0.4 fusion.7
  101.2 0.5 copy-done.9
  101.7 0.5 fusion.6
  102.1 0.5 fusion.5
  102.6 0.5 fusion.2
  103.1 1.5 %fusion.1 = bf16[1,2048,256]{2,1,0:T(8,128)(2,1)} fusion(bf16[256,2048]{1,0:T(8,128)(2,1)S(1)} %bitcast.110, bf16[256,256]{1,0:T(8,128)(2,1)S(1)} %get-tuple-element.16), kind=kOutput, calls=%fused_computation.12 | convolution fusion | flops 268959744 | bytes 2228224 | tf_op jit(solution)/shard_map/sd,sf->df/dot_general | solution.py:80
  104.6 1.5 %fusion.4 = bf16[1,2048,256]{2,1,0:T(8,128)(2,1)} fusion(bf16[256,2048]{1,0:T(8,128)(2,1)S(1)} %bitcast.111, bf16[256,256]{1,0:T(8,128)(2,1)S(1)} %get-tuple-element.13), kind=kOutput, calls=%fused_computation.15 | convolution fusion | flops 268959744 | bytes 2228224 | tf_op jit(solution)/shard_map/sd,sf->df/dot_general | solution.py:85
  106.0 1.5 %pad_maximum_fusion.2 = bf16[2,256,2048]{2,1,0:T(8,128)(2,1)} fusion(bf16[1,256,2048]{2,1,0:T(8,128)(2,1)S(1)} %fusion.6, bf16[1,256,2048]{2,1,0:T(8,128)(2,1)S(1)} %fusion.5), kind=kLoop, calls=%fused_computation.20 | loop fusion | flops 1048576 | bytes 4194304 | tf_op jit(solution)/shard_map/stack | solution.py:132
  107.5 15.4 %reduce-scatter.2.cloned.1.call-done = bf16[256,512]{1,0:T(8,128)(2,1)} async-done(((bf16[256,2048]{1,0:T(8,128)(2,1)}), bf16[256,512]{1,0:T(8,128)(2,1)}) %reduce-scatter.2.cloned.1.call-update) | async-done | bytes 262160 | tf_op jit(solution)/shard_map/reduce_scatter | solution.py:96
  122.9 5.5 %all-to-all-start.3 = ((bf16[8,32,512]{2,1,0:T(8,128)(2,1)}), bf16[8,32,512]{2,1,0:T(8,128)(2,1)S(1)}, u32[]{:S(2)}, u32[]{:S(2)}) async-start(bf16[8,32,512]{2,1,0:T(8,128)(2,1)} %bitcast.120), calls=%async_computation.4 | async-start | bytes 524288 | tf_op jit(solution)/shard_map/all_to_all | solution.py:100
  128.5 0.5 fusion.3
  129.0 0.7 copy-done.3
  129.7 0.3 copy-done.4
  130.0 2.4 %pad_maximum_fusion = (bf16[2,2048,256]{2,1,0:T(8,128)(2,1)}, bf16[2,2048,256]{2,1,0:T(8,128)(2,1)}) fusion(bf16[1,2048,256]{2,1,0:T(8,128)(2,1)S(1)} %fusion.2, bf16[1,2048,256]{2,1,0:T(8,128)(2,1)S(1)} %copy-done.3, bf16[1,2048,256]{2,1,0:T(8,128)(2,1)S(1)} %copy-done.4, bf16[1,2048,256]{2,1,0:T(8,128)(2,1)S(1)} %fusion.3), kind=kLoop, calls=%fused_computation.18 | loop fusion | flops 2097152 | bytes 8388608 | tf_op jit(solution)/shard_map/stack | solution.py:130
  132.4 4.8 %all-to-all-done.3 = bf16[8,32,512]{2,1,0:T(8,128)(2,1)S(1)} async-done(((bf16[8,32,512]{2,1,0:T(8,128)(2,1)}), bf16[8,32,512]{2,1,0:T(8,128)(2,1)S(1)}, u32[]{:S(2)}, u32[]{:S(2)}) %all-to-all-start.3) | async-done | bytes 262176 | tf_op jit(solution)/shard_map/all_to_all | solution.py:100
  137.2 0.9 convolution_convert_fusion.8
  (29 shorter events, 0.1 us)
Async XLA Ops:
  7.2 1.7 %copy-start = (bf16[168,2048]{1,0:T(8,128)(2,1)S(1)}, bf16[168,2048]{1,0:T(8,128)(2,1)}, u32[]{:S(2)}) copy-start(bf16[168,2048]{1,0:T(8,128)(2,1)} %param.8) | copy-start | bytes 2064388
  7.2 33.9 %all-gather.5.cloned.1.call-start = ((), (), s32[]{:S(2)}) async-start(), calls=%async_computation.7 | async-start | bytes 1310720 | tf_op jit(solution)/shard_map/all_gather | solution.py:45
  25.2 34.1 %all-gather.3.cloned.1.call-start = ((), (), s32[]{:S(2)}) async-start(), calls=%async_computation.6 | async-start | bytes 1310720 | tf_op jit(solution)/shard_map/all_gather | solution.py:46
  41.1 2.1 %copy-start.1 = (bf16[8,32,2048]{2,1,0:T(8,128)(2,1)S(1)}, bf16[8,32,2048]{2,1,0:T(8,128)(2,1)}, u32[]{:S(2)}) copy-start(bf16[8,32,2048]{2,1,0:T(8,128)(2,1)} %all-gather.5.cloned.1.call-done) | copy-start | bytes 3145732
  41.1 3.8 %copy-start.6 = (bf16[2,2048,256]{2,1,0:T(8,128)(2,1)S(1)}, bf16[2,2048,256]{2,1,0:T(8,128)(2,1)}, u32[]{:S(2)}) copy-start(bf16[2,2048,256]{2,1,0:T(8,128)(2,1)} %param.14) | copy-start | bytes 6291460
  44.9 1.2 copy-start.13
  47.2 16.1 %copy-start.8 = (bf16[256,256]{1,0:T(8,128)(2,1)}, bf16[256,256]{1,0:T(8,128)(2,1)S(1)}, u32[]{:S(2)}) copy-start(bf16[256,256]{1,0:T(8,128)(2,1)S(1)} %get-tuple-element.19) | copy-start | bytes 393220
  59.4 2.2 %copy-start.2 = (bf16[8,32,2048]{2,1,0:T(8,128)(2,1)S(1)}, bf16[8,32,2048]{2,1,0:T(8,128)(2,1)}, u32[]{:S(2)}) copy-start(bf16[8,32,2048]{2,1,0:T(8,128)(2,1)} %all-gather.3.cloned.1.call-done) | copy-start | bytes 3145732
  61.5 14.2 %copy-start.11 = (bf16[168,2]{0,1:T(2,128)(2,1)S(1)}, bf16[168,2]{0,1:T(2,128)(2,1)}, u32[]{:S(2)}) copy-start(bf16[168,2]{0,1:T(2,128)(2,1)} %param.12) | copy-start | bytes 2020
  61.5 20.9 %copy-start.10 = (s32[168,2]{0,1:T(2,128)S(1)}, s32[168,2]{0,1:T(2,128)}, u32[]{:S(2)}) copy-start(s32[168,2]{0,1:T(2,128)} %param.11) | copy-start | bytes 4036
  70.0 12.2 %all-to-all-start.4 = ((f32[8,32,2]{1,2,0:T(2,128)}), f32[8,32,2]{1,2,0:T(2,128)S(1)}, u32[]{:S(2)}, u32[]{:S(2)}) async-start(f32[8,32,2]{1,2,0:T(2,128)} %psum.7), calls=%async_computation.5 | async-start | bytes 16384 | tf_op jit(solution)/shard_map/all_to_all | solution.py:107
  75.7 47.3 %reduce-scatter.2.cloned.1.call-start = ((), (), s32[]{:S(2)}) async-start(), calls=%async_computation.8 | async-start | bytes 1310720 | tf_op jit(solution)/shard_map/reduce_scatter | solution.py:96
  92.5 1.6 %copy-start.12 = (bf16[2,256,2048]{2,1,0:T(8,128)(2,1)S(1)}, bf16[2,256,2048]{2,1,0:T(8,128)(2,1)}, u32[]{:S(2)}) copy-start(bf16[2,256,2048]{2,1,0:T(8,128)(2,1)} %param.15) | copy-start | bytes 6291460
  94.1 1.7 %copy-start.5 = (bf16[2,2048,256]{2,1,0:T(8,128)(2,1)S(1)}, bf16[2,2048,256]{2,1,0:T(8,128)(2,1)}, u32[]{:S(2)}) copy-start(bf16[2,2048,256]{2,1,0:T(8,128)(2,1)} %param.13) | copy-start | bytes 6291460
  95.7 1.6 %copy-start.7 = (bf16[2,2048,256]{2,1,0:T(8,128)(2,1)S(1)}, bf16[2,2048,256]{2,1,0:T(8,128)(2,1)}, u32[]{:S(2)}) copy-start(bf16[2,2048,256]{2,1,0:T(8,128)(2,1)} %param.14) | copy-start | bytes 6291460
  97.3 0.9 copy-start.14
  97.3 1.0 copy-start.15
  100.8 0.9 copy-start.9
  122.9 14.3 %all-to-all-start.3 = ((bf16[8,32,512]{2,1,0:T(8,128)(2,1)}), bf16[8,32,512]{2,1,0:T(8,128)(2,1)S(1)}, u32[]{:S(2)}, u32[]{:S(2)}) async-start(bf16[8,32,512]{2,1,0:T(8,128)(2,1)} %bitcast.120), calls=%async_computation.4 | async-start | bytes 524288 | tf_op jit(solution)/shard_map/all_to_all | solution.py:100
  128.5 1.2 copy-start.3
  128.5 1.5 %copy-start.4 = (bf16[1,2048,256]{2,1,0:T(8,128)(2,1)S(1)}, bf16[1,2048,256]{2,1,0:T(8,128)(2,1)}, u32[]{:S(2)}) copy-start(bf16[1,2048,256]{2,1,0:T(8,128)(2,1)} %fusion.4) | copy-start | bytes 3145732
Sparse Core Ops, SparseCore 0:
  25.4 15.6 all-gather.4
  42.7 16.6 all-gather.2
  100.9 22.0 reduce-scatter.1
where the time goes:
time: 145 us
  blocking collectives  43.6 us (30%)
  waiting for transfers between devices  41.5 us (29%)
  matrix products  23.3 us (16%)
  between operations  14 us (10%)
  starting transfers between devices  11.3 us (8%)
  other arithmetic  6 us (4%)
  local copies, waits for them, and re-layouts  5 us (3%)
    all_to_all x1, blocking collectives, on_device(): lax.all_to_all(arrange(part_x), 'ep', split_axis=0, concat_axis=0, tiled=...  16.1 us
    reduce_scatter x1, waiting for transfers between devices, on_device(): lax.psum_scatter(dx_total.astype(jnp.bfloat16), 'tp', scatter_dimension=1...  15.4 us
    all_gather x1, waiting for transfers between devices, on_device(): lax.all_gather(thin_dy, 'tp', axis=2, tiled=True)  12.2 us
    all_to_all x1, blocking collectives, on_device(): lax.all_to_all(arrange(part_dy), 'ep', split_axis=0, concat_axis=0, tiled...  12.1 us
    all_to_all x1, blocking collectives, on_device(): lax.all_to_all(arrange(combine), 'ep', split_axis=0, concat_axis=0, tiled...  8.86 us
    psum x1, blocking collectives, on_device(): gate_sum = lax.psum(gate_part, 'tp')  6.55 us
    all_to_all x1, waiting for transfers between devices, on_device(): lax.all_to_all(gate_sum.reshape(ep_count, capacity, experts_here), 'ep',...  6.45 us
    all_to_all x1, starting transfers between devices, on_device(): lax.all_to_all(gate_sum.reshape(ep_count, capacity, experts_here), 'ep',...  5.68 us
  transfers between devices with their start and end apart: 5, of which 5 were waited for; matrix products, arithmetic and copies ran while one was open for 11% of the time, Pallas kernels for 0%

commit v1 on v0

v1 whole, which is shorter than its diff:
```python
import functools

import jax
import jax.numpy as jnp
from jax import lax
from jax.experimental import pallas as pl
from jax.experimental.pallas import tpu as pltpu
from jax.sharding import PartitionSpec as P

MESH = pl.DeviceIdType.MESH
LANES = 128
NT = (((1,), (1,)), ((), ()))
TN = (((0,), (0,)), ((), ()))
NN = (((1,), (0,)), ((), ()))


def dot(a, b, dims=NN):
    return lax.dot_general(a, b, dims, preferred_element_type=jnp.float32)


def each(count, body):
    if count <= 8:
        for i in range(count):
            body(i)
    else:
        lax.fori_loop(0, count, lambda i, c: (body(i), c)[1], 0)


def aligned(value, step):
    return value if isinstance(value, int) else pl.multiple_of(value, step)


def kernel(
    ep, tp, cap,
    tok_ref, cot_ref, gid_ref, wid_ref, gw_ref, wg_ref, wu_ref, wd_ref,
    dtok_ref, dgate_ref, gwg_ref, gwu_ref, gwd_ref,
    src, placed, rows_in, wg, wu, wd, acc, gate_b, up_b, act_c,
    to_partner, from_partner, dx_acc, to_x, from_x, to_ep, back,
    gate_in, gate_sum, gate_back, vwg, vwu, vwd,
    load_sem, out_sem, own_sem, send1, recv_rows, send_x, send_p, send_p2,
    dxp_send, dxp_recv, dxx_send, dxx_recv, dxe_send, dxe_recv,
    gt_send, gt_recv, ge_send, ge_recv,
):
    e_me = lax.axis_index("ep")
    t_me = lax.axis_index("tp")
    core = lax.rem(t_me, 2)
    x_me = lax.div(t_me, 2)
    partner = t_me + 1 - 2 * core
    nx = tp // 2
    tok_rows, width = tok_ref.shape
    cs = width // tp
    slots = ep * cap
    experts = wg.shape[0]
    bf16 = jnp.bfloat16

    barrier = pltpu.get_barrier_semaphore()
    each(ep - 1, lambda i: pl.semaphore_signal(
        barrier, inc=1, device_id=(lax.rem(e_me + 1 + i, ep), t_me), device_id_type=MESH))
    each(tp - 1, lambda i: pl.semaphore_signal(
        barrier, inc=1, device_id=(e_me, lax.rem(t_me + 1 + i, tp)), device_id_type=MESH))

    my_cols = pl.ds(pl.multiple_of(t_me * cs, LANES), cs)
    loads = [
        pltpu.make_async_copy(tok_ref.at[:, my_cols], src.at[:, pl.ds(0, cs)], load_sem.at[0]),
        pltpu.make_async_copy(cot_ref.at[:, my_cols], src.at[:, pl.ds(cs, cs)], load_sem.at[1]),
        pltpu.make_async_copy(wg_ref, wg, load_sem.at[2]),
        pltpu.make_async_copy(wu_ref, wu, load_sem.at[3]),
        pltpu.make_async_copy(wd_ref, wd, load_sem.at[4]),
    ]
    for load in loads:
        load.start()

    group = gid_ref[...]
    in_group = (group == lax.broadcasted_iota(jnp.int32, (tok_rows, LANES), 1)).astype(jnp.float32)
    earlier = (
        lax.broadcasted_iota(jnp.int32, (tok_rows, tok_rows), 0)
        > lax.broadcasted_iota(jnp.int32, (tok_rows, tok_rows), 1)
    ).astype(jnp.float32).astype(bf16)
    before = dot(earlier, in_group.astype(bf16))
    rank = jnp.sum(before * in_group, axis=1, keepdims=True).astype(jnp.int32)
    slot_lane = lax.broadcasted_iota(jnp.int32, (tok_rows, slots), 1)
    place = (slot_lane == group * cap + rank).astype(jnp.float32).astype(bf16)
    lane = lax.broadcasted_iota(jnp.int32, (tok_rows, LANES), 1)
    weights = gw_ref[...].astype(jnp.float32)
    comb = jnp.zeros((tok_rows, LANES), jnp.float32)
    for k in range(weights.shape[1]):
        comb = comb + jnp.where(lane == wid_ref[:, k : k + 1], weights[:, k : k + 1], 0.0)
    src[:, pl.ds(2 * cs, LANES)] = comb.astype(bf16)
    loads[0].wait()
    loads[1].wait()
    placed[...] = dot(place, src[...], TN).astype(bf16)

    pl.semaphore_wait(barrier, ep + tp - 2)

    def block(e):
        return pl.ds(aligned(e * cap, 16), cap)

    distances = list(range(ep))
    if ep <= 8:
        distances = [0]
        for k in range(1, ep // 2 + 1):
            distances += sorted({k, ep - k})

    def stage1(d):
        g = lax.rem(e_me + d, ep)
        return pltpu.make_async_remote_copy(
            src_ref=placed.at[block(g)], dst_ref=rows_in.at[t_me, block(e_me)],
            send_sem=send1.at[d], recv_sem=recv_rows.at[t_me, e_me],
            device_id=(g, t_me), device_id_type=MESH)

    own = pltpu.make_async_copy(
        placed.at[block(e_me)], rows_in.at[t_me, block(e_me)], own_sem.at[0])
    own.start()
    if ep <= 8:
        for d in distances[1:]:
            stage1(d).start()
    else:
        each(ep - 1, lambda i: stage1(i + 1).start())

    def arrived(q, e, cols):
        part = rows_in.at[q, block(e), pl.ds(0, cols)]
        pltpu.make_async_remote_copy(
            src_ref=part, dst_ref=part, send_sem=send1.at[0], recv_sem=recv_rows.at[q, e],
            device_id=(e_me, partner), device_id_type=MESH).wait_recv()

    def forward(q, e, sem, target):
        part = rows_in.at[q, block(e), pl.ds(0, 2 * cs)]
        return pltpu.make_async_remote_copy(
            src_ref=part, dst_ref=part, send_sem=sem, recv_sem=recv_rows.at[q, e],
            device_id=(e_me, target), device_id_type=MESH)

    def x_peer(k):
        return lax.rem(x_me + k, nx) * 2 + core

    def to_peers(d):
        e = lax.rem(e_me - d + ep, ep)
        copies = [forward(t_me, e, send_x.at[k - 1, d], x_peer(k)) for k in range(1, nx)]
        return copies + [forward(t_me, e, send_p.at[d], partner)]

    def stage2(d):
        for copy in to_peers(d):
            copy.start()

    def relays(d):
        e = lax.rem(e_me - d + ep, ep)
        return [(x_peer(k), e, forward(x_peer(k), e, send_p2.at[k - 1, d], partner))
                for k in range(1, nx)]

    def stage3(d):
        for q, e, copy in relays(d):
            arrived(q, e, 2 * cs)
            copy.start()

    own.wait()
    stage2(0)
    if ep <= 8:
        for i, d in enumerate(distances[1:]):
            arrived(t_me, lax.rem(e_me - d + ep, ep), 2 * cs + LANES)
            stage2(d)
            stage3(distances[i])
    else:
        def later(i):
            arrived(t_me, lax.rem(e_me - i - 1 + ep, ep), 2 * cs + LANES)
            stage2(i + 1)
        each(ep - 1, later)
        each(ep - 1, stage3)

    for load in loads[2:]:
        load.wait()

    def share(q):
        return pl.ds(aligned(q * cs, LANES), cs)

    def hidden(q, first):
        xq = rows_in[q, :, pl.ds(0, cs)]
        yq = rows_in[q, :, pl.ds(cs, cs)]
        for e in range(experts):
            for n, value in enumerate((
                dot(xq, wg[e, share(q), :]),
                dot(xq, wu[e, share(q), :]),
                dot(yq, wd[e, :, share(q)], NT),
            )):
                acc[e, n] = value if first else acc[e, n] + value

    def all_arrived(q):
        each(ep, lambda e: arrived(q, e, 2 * cs))

    hidden(t_me, True)
    stage3(distances[-1])
    all_arrived(partner)
    hidden(partner, False)

    def x_quarters(k):
        hidden(x_peer(k), False)
        other = lax.rem(x_me + k, nx) * 2 + 1 - core
        all_arrived(other)
        hidden(other, False)
    each(nx - 1, lambda i: x_quarters(i + 1))

    row8 = lax.broadcasted_iota(jnp.int32, (8, slots), 0)
    gates = jnp.zeros((8, slots), jnp.float32)
    for e in range(experts):
        pre_gate, pre_up, dy_down = acc[e, 0], acc[e, 1], acc[e, 2]
        c = rows_in[t_me, :, pl.ds(2 * cs, LANES)][:, e : e + 1].astype(jnp.float32)
        sig = jax.nn.sigmoid(pre_gate)
        silu = pre_gate * sig
        act = silu * pre_up
        prod = act.astype(bf16).astype(jnp.float32) * dy_down
        act_grad = c * dy_down
        act_c[e] = (c * act).astype(bf16)
        gate_b[e] = (act_grad * pre_up * sig * (1.0 + pre_gate * (1.0 - sig))).astype(bf16)
        up_b[e] = (act_grad * silu).astype(bf16)
        high = prod.astype(bf16)
        low = (prod - high.astype(jnp.float32)).astype(bf16)
        ones = jnp.ones((8, prod.shape[1]), bf16)
        gates = gates + jnp.where(row8 == e, dot(ones, high, NT) + dot(ones, low, NT), 0.0)
    gate_in[t_me] = gates

    def gate_tp(i):
        return pltpu.make_async_remote_copy(
            src_ref=gate_in.at[t_me], dst_ref=gate_in.at[t_me],
            send_sem=gt_send.at[i], recv_sem=gt_recv.at[t_me],
            device_id=(e_me, lax.rem(t_me + 1 + i, tp)), device_id_type=MESH)

    def dx_of(q):
        total = None
        for e in range(experts):
            part = dot(gate_b[e], wg[e, share(q), :], NT) + dot(up_b[e], wu[e, share(q), :], NT)
            total = part if total is None else total + part
        return total

    def dx_partner(k):
        return pltpu.make_async_remote_copy(
            src_ref=to_partner.at[k], dst_ref=from_partner.at[k],
            send_sem=dxp_send.at[k], recv_sem=dxp_recv.at[k],
            device_id=(e_me, partner), device_id_type=MESH)

    def give_partner(i):
        k = nx - 1 - i
        to_partner[k] = dx_of(lax.rem(x_me + k, nx) * 2 + 1 - core).astype(bf16)
        dx_partner(k).start()
    each(nx, give_partner)
    each(tp - 1, lambda i: gate_tp(i).start())

    def dx_x(k, d):
        e = lax.rem(e_me + d, ep)
        return pltpu.make_async_remote_copy(
            src_ref=to_x.at[k - 1, block(e)], dst_ref=from_x.at[k - 1, block(e)],
            send_sem=dxx_send.at[k - 1, d], recv_sem=dxx_recv.at[k - 1, d],
            device_id=(e_me, x_peer(k)), device_id_type=MESH)

    far = distances[::-1]

    def walk(body):
        if ep <= 8:
            for i, d in enumerate(far):
                body(i, d)
        else:
            each(ep, lambda i: body(i, ep - 1 - i))

    def give_x(k):
        mine = dx_of(x_peer(k))
        dx_partner(k).wait_recv()
        to_x[k - 1] = (mine + from_partner[k].astype(jnp.float32)).astype(bf16)
        walk(lambda i, d: dx_x(k, d).start())
    each(nx - 1, lambda i: give_x(i + 1))
    mine = dx_of(t_me)
    dx_partner(0).wait_recv()
    dx_acc[...] = mine + from_partner[0].astype(jnp.float32)

    def gate_ep(d):
        return pltpu.make_async_remote_copy(
            src_ref=gate_sum, dst_ref=gate_back.at[e_me],
            send_sem=ge_send.at[d], recv_sem=ge_recv.at[e_me],
            device_id=(lax.rem(e_me + d, ep), t_me), device_id_type=MESH)

    def gate_wait(i):
        q = lax.rem(t_me + 1 + i, tp)
        pltpu.make_async_remote_copy(
            src_ref=gate_in.at[q], dst_ref=gate_in.at[q],
            send_sem=gt_send.at[i], recv_sem=gt_recv.at[q],
            device_id=(e_me, q), device_id_type=MESH).wait_recv()
    each(tp - 1, gate_wait)
    total = gate_in[0]
    for q in range(1, tp):
        total = total + gate_in[q]
    gate_sum[...] = total
    gate_back[e_me] = total
    each(ep - 1, lambda i: gate_ep(i + 1).start())

    def outs(q):
        cols = share(q)
        return [
            pltpu.make_async_copy(vwg.at[:, cols, :], gwg_ref.at[:, cols, :], out_sem.at[q, 0]),
            pltpu.make_async_copy(vwu.at[:, cols, :], gwu_ref.at[:, cols, :], out_sem.at[q, 1]),
            pltpu.make_async_copy(vwd.at[:, :, cols], gwd_ref.at[:, :, cols], out_sem.at[q, 2]),
        ]

    def weight_grads(q):
        x_t = rows_in[q, :, pl.ds(0, cs)].T
        yq = rows_in[q, :, pl.ds(cs, cs)]
        for e in range(experts):
            vwg[e, share(q), :] = dot(x_t, gate_b[e]).astype(bf16)
            vwu[e, share(q), :] = dot(x_t, up_b[e]).astype(bf16)
            vwd[e, :, share(q)] = dot(act_c[e], yq, TN).astype(bf16)
        for copy in outs(q):
            copy.start()

    def dx_ep(d):
        g = lax.rem(e_me + d, ep)
        return pltpu.make_async_remote_copy(
            src_ref=to_ep.at[block(g)], dst_ref=back.at[block(e_me)],
            send_sem=dxe_send.at[d], recv_sem=dxe_recv.at[e_me],
            device_id=(g, t_me), device_id_type=MESH)

    def finish_chunk(d):
        rows = block(lax.rem(e_me + d, ep))
        value = dx_acc[rows, :]
        for k in range(1, nx):
            dx_x(k, d).wait_recv()
            value = value + from_x[k - 1, rows, :].astype(jnp.float32)
        return value.astype(bf16)

    def chunk(i, d):
        to_ep[block(lax.rem(e_me + d, ep)), :] = finish_chunk(d)
        dx_ep(d).start()

    if ep <= 8:
        done = 0
        for i, d in enumerate(far[:-1]):
            chunk(i, d)
            if i % 2 == 0 and done < tp:
                weight_grads(done)
                done += 1
        for q in range(done, tp):
            weight_grads(q)
    else:
        each(ep - 1, lambda i: chunk(i, ep - 1 - i))
        each(tp, weight_grads)
    back[block(e_me), :] = finish_chunk(0)

    def gate_arrived(i):
        g = lax.rem(e_me + 1 + i, ep)
        pltpu.make_async_remote_copy(
            src_ref=gate_sum, dst_ref=gate_back.at[g],
            send_sem=ge_send.at[0], recv_sem=ge_recv.at[g],
            device_id=(g, t_me), device_id_type=MESH).wait_recv()
    each(ep - 1, gate_arrived)
    pick = (slot_lane == e_me * cap + rank).astype(jnp.float32).astype(bf16)
    sums = gate_back[...].reshape(ep * 8, slots)
    high = sums.astype(bf16)
    low = (sums - high.astype(jnp.float32)).astype(bf16)
    dense = dot(pick, high, NT) + dot(pick, low, NT)
    row_lane = lax.broadcasted_iota(jnp.int32, (tok_rows, ep * 8), 1)
    for k in range(weights.shape[1]):
        wanted = row_lane == group * 8 + wid_ref[:, k : k + 1]
        dgate_ref[:, k : k + 1] = jnp.sum(jnp.where(wanted, dense, 0.0), axis=1, keepdims=True)

    def back_arrived(i):
        g = lax.rem(e_me + 1 + i, ep)
        pltpu.make_async_remote_copy(
            src_ref=to_ep.at[block(g)], dst_ref=back.at[block(g)],
            send_sem=dxe_send.at[0], recv_sem=dxe_recv.at[g],
            device_id=(g, t_me), device_id_type=MESH).wait_recv()
    each(ep - 1, back_arrived)
    dtok_ref[...] = dot(place, back[...]).astype(bf16)

    def sent1(i):
        d = i + 1
        stage1(d).wait_send()
        gate_ep(d).wait_send()
        dx_ep(d).wait_send()
    each(ep - 1, sent1)

    def sent2(d):
        for copy in to_peers(d):
            copy.wait_send()
        for _, _, copy in relays(d):
            copy.wait_send()
        for k in range(1, nx):
            dx_x(k, d).wait_send()
    each(ep, sent2)
    each(nx, lambda k: dx_partner(k).wait_send())
    each(tp - 1, lambda i: gate_tp(i).wait_send())

    def written(q):
        for copy in outs(q):
            copy.wait()
    each(tp, written)


def on_device(tokens, cotangent, group_ids, within_ids, gate_weights, w_gate, w_up, w_down):
    ep = lax.axis_size("ep")
    tp = lax.axis_size("tp")
    tok_rows, width = tokens.shape
    experts, _, ff = w_gate.shape
    cap = (3 * tok_rows + 2 * ep - 1) // (2 * ep)
    cap = -(-cap // 16) * 16
    slots = ep * cap
    cs = width // tp
    nx = tp // 2
    bf16, f32 = jnp.bfloat16, jnp.float32
    dma = pltpu.SemaphoreType.DMA
    anywhere = pl.BlockSpec(memory_space=pl.ANY)
    vmem = pl.BlockSpec(memory_space=pltpu.VMEM)
    scratch = [
        pltpu.VMEM((tok_rows, 2 * cs + LANES), bf16),
        pltpu.VMEM((slots, 2 * cs + LANES), bf16),
        pltpu.VMEM((tp, slots, 2 * cs + LANES), bf16),
        pltpu.VMEM(w_gate.shape, bf16),
        pltpu.VMEM(w_up.shape, bf16),
        pltpu.VMEM(w_down.shape, bf16),
        pltpu.VMEM((experts, 3, slots, ff), f32),
        pltpu.VMEM((experts, slots, ff), bf16),
        pltpu.VMEM((experts, slots, ff), bf16),
        pltpu.VMEM((experts, slots, ff), bf16),
        pltpu.VMEM((nx, slots, cs), bf16),
        pltpu.VMEM((nx, slots, cs), bf16),
        pltpu.VMEM((slots, cs), f32),
        pltpu.VMEM((nx - 1, slots, cs), bf16),
        pltpu.VMEM((nx - 1, slots, cs), bf16),
        pltpu.VMEM((slots, cs), bf16),
        pltpu.VMEM((slots, cs), bf16),
        pltpu.VMEM((tp, 8, slots), f32),
        pltpu.VMEM((8, slots), f32),
        pltpu.VMEM((ep, 8, slots), f32),
        pltpu.VMEM(w_gate.shape, bf16),
        pltpu.VMEM(w_up.shape, bf16),
        pltpu.VMEM(w_down.shape, bf16),
        dma((5,)), dma((tp, 3)), dma((1,)), dma((ep,)), dma((tp, ep)),
        dma((nx - 1, ep)), dma((ep,)), dma((nx - 1, ep)),
        dma((nx,)), dma((nx,)), dma((nx - 1, ep)), dma((nx - 1, ep)), dma((ep,)), dma((ep,)),
        dma((tp,)), dma((tp,)), dma((ep,)), dma((ep,)),
    ]
    return pl.pallas_call(
        functools.partial(kernel, ep, tp, cap),
        out_shape=(
            jax.ShapeDtypeStruct((tok_rows, cs), bf16),
            jax.ShapeDtypeStruct(within_ids.shape, f32),
            jax.ShapeDtypeStruct(w_gate.shape, bf16),
            jax.ShapeDtypeStruct(w_up.shape, bf16),
            jax.ShapeDtypeStruct(w_down.shape, bf16),
        ),
        in_specs=[anywhere, anywhere, vmem, vmem, vmem, anywhere, anywhere, anywhere],
        out_specs=(vmem, vmem, anywhere, anywhere, anywhere),
        scratch_shapes=scratch,
        compiler_params=pltpu.CompilerParams(
            collective_id=0, has_side_effects=True, vmem_limit_bytes=56 * 1024 * 1024),
    )(tokens, cotangent, group_ids, within_ids, gate_weights, w_gate, w_up, w_down)


def solution(mesh):
    in_specs = (
        P("ep", None),
        P("ep", None),
        P("ep", None),
        P("ep", None),
        P("ep", None),
        P("ep", None, "tp"),
        P("ep", None, "tp"),
        P("ep", "tp", None),
    )
    out_specs = (
        P("ep", "tp"),
        P("ep", None),
        P("ep", None, "tp"),
        P("ep", None, "tp"),
        P("ep", "tp", None),
    )
    return jax.shard_map(
        on_device, mesh=mesh, in_specs=in_specs, out_specs=out_specs, check_vma=False
    )
```

time: 145 us -> 58.9 us (0.41)
  Pallas kernels: 0 us -> 43.7 us
  blocking collectives: 43.6 us -> 0 us
  waiting for transfers between devices: 41.5 us -> 0 us
  matrix products: 23.3 us -> 0 us
  between operations: 14 us -> 0.64 us
  starting transfers between devices: 11.3 us -> 0 us
  local copies, waits for them, and re-layouts: 5 us -> 14.3 us
  other arithmetic: 6 us -> 0 us
    pallas_call x0 -> x1, Pallas kernels: none -> 43.7 us  [on_device(): pl.pallas_call(functools.partial(kernel, ep, tp, cap), out_shape=(jax.Sha...]
    all_to_all x3 -> x0, blocking collectives: 37 us -> none  [the longest x1 16.1 us: on_device(): lax.all_to_all(arrange(part_x), 'ep', split_axis=0, concat_axis=0, tiled=...]
    dot_general x24 -> x0, matrix products: 23.3 us -> none  [the longest x2 3.9 us: on_device(): jnp.dot(act_b, w_down[expert], preferred_element_type=jnp.float32)]
    reduce_scatter x1 -> x0, waiting for transfers between devices: 15.4 us -> none  [on_device(): lax.psum_scatter(dx_total.astype(jnp.bfloat16), 'tp', scatter_dimension=1...]
    all_gather x2 -> x0, waiting for transfers between devices: 14.7 us -> none  [the longest x1 12.2 us: on_device(): lax.all_gather(thin_dy, 'tp', axis=2, tiled=True)]
    all_to_all x2 -> x0, waiting for transfers between devices: 11.3 us -> none  [the longest x1 6.45 us: on_device(): lax.all_to_all(gate_sum.reshape(ep_count, capacity, experts_here), 'ep',...]
    all_to_all x2 -> x0, starting transfers between devices: 11.2 us -> none  [the longest x1 5.68 us: on_device(): lax.all_to_all(gate_sum.reshape(ep_count, capacity, experts_here), 'ep',...]
    unnamed x32 -> x11, local copies, waits for them, and re-layouts: 4.49 us -> 12.7 us
  transfers between devices with their start and end apart: 5 -> 0, of which waited for: 5 -> 0; matrix products, arithmetic and copies ran while one was open for 11% -> 0% of each run, Pallas kernels for 0% -> 0%
where the time goes in v1:
time: 58.9 us; the launch traced here: 58.6 us
  Pallas kernels  43.7 us (74%)
  local copies, waits for them, and re-layouts  14.3 us (24%)
  between operations  0.64 us (1%)
    pallas_call x1, Pallas kernels, on_device(): pl.pallas_call(functools.partial(kernel, ep, tp, cap), out_shape=(jax.Sha...  43.7 us
    unnamed x11, local copies, waits for them, and re-layouts  12.7 us
    pallas_call x1, local copies, waits for them, and re-layouts, on_device(): pl.pallas_call(functools.partial(kernel, ep, tp, cap), out_shape=(jax.Sha...  1.55 us

profile of v1, /device:TPU:0, one launch (start us, length us, event | category | flops | bytes accessed | tf_op | source)
XLA Modules:
  0.0 58.6 jit_solution(8795621366214708523)
XLA Ops:
  0.6 1.4 %copy.15.gw_ref = bf16[168,2]{1,0:T(8,128)(2,1)} copy(bf16[168,2]{0,1:T(2,128)(2,1)} %param.12) | data formatting | bytes 1344 | tf_op args[4]
  2.1 1.4 %copy.13.gid_ref = s32[168,1]{1,0:T(8,128)} copy(s32[168,1]{0,1:T(1,128)} %param.10) | data formatting | bytes 1344 | tf_op args[2]
  3.5 1.4 %copy.14.wid_ref = s32[168,2]{1,0:T(8,128)} copy(s32[168,2]{0,1:T(2,128)} %param.11) | data formatting | bytes 2688 | tf_op args[3]
  4.9 43.7 %shard_map.119 = (bf16[168,512]{1,0:T(8,128)(2,1)}, f32[168,2]{1,0:T(8,128)}, bf16[2,2048,256]{2,1,0:T(8,128)(2,1)}, bf16[2,2048,256]{2,1,0:T(8,128)(2,1)}, bf16[2,256,2048]{2,1,0:T(8,128)(2,1)}) custom-call(bf16[168,2048]{1,0:T(8,128)(2,1)} %tok_ref.1, bf16[168,2048]{1,0:T(8,128)(2,1)} %cot_ref.1, s32[168,1]{1,0:T(8,128)} %copy.13.gid_ref, ...), custom_call_target="tpu_custom_call" | custom-call | tf_op jit(solution)/shard_map/pallas_call | solution.py:435
  48.6 1.5 %copy.16 = f32[168,2]{0,1:T(2,128)} copy(f32[168,2]{1,0:T(8,128)} %get-tuple-element.6) | data formatting | bytes 2688 | tf_op jit(solution)/shard_map/pallas_call | solution.py:435
  50.2 1.6 %copy.21 = bf16[168,512]{1,0:T(8,128)(2,1)} copy(bf16[168,512]{1,0:T(8,128)(2,1)} %get-tuple-element.15) | data formatting | bytes 344064
  51.8 0.0 copy-start.1
  51.8 3.2 %copy.22 = bf16[2,2048,256]{2,1,0:T(8,128)(2,1)} copy(bf16[2,2048,256]{2,1,0:T(8,128)(2,1)} %get-tuple-element.17) | data formatting | bytes 4194304
  55.0 0.0 copy-done.1
  55.0 0.0 copy-start
  55.0 1.3 %copy.23 = bf16[2,2048,256]{2,1,0:T(8,128)(2,1)} copy(bf16[2,2048,256]{2,1,0:T(8,128)(2,1)S(1)} %copy-done.1) | data formatting | bytes 4194304
  56.3 1.0 %copy-done = bf16[2,256,2048]{2,1,0:T(8,128)(2,1)S(1)} copy-done((bf16[2,256,2048]{2,1,0:T(8,128)(2,1)S(1)}, bf16[2,256,2048]{2,1,0:T(8,128)(2,1)}, u32[]{:S(2)}) %copy-start) | copy-done | bytes 2097176
  57.3 1.3 %copy.24 = bf16[2,256,2048]{2,1,0:T(8,128)(2,1)} copy(bf16[2,256,2048]{2,1,0:T(8,128)(2,1)S(1)} %copy-done) | data formatting | bytes 4194304
Async XLA Ops:
  51.8 3.2 %copy-start.1 = (bf16[2,2048,256]{2,1,0:T(8,128)(2,1)S(1)}, bf16[2,2048,256]{2,1,0:T(8,128)(2,1)}, u32[]{:S(2)}) copy-start(bf16[2,2048,256]{2,1,0:T(8,128)(2,1)} %get-tuple-element.18) | copy-start | bytes 6291460
  55.0 2.3 %copy-start = (bf16[2,256,2048]{2,1,0:T(8,128)(2,1)S(1)}, bf16[2,256,2048]{2,1,0:T(8,128)(2,1)}, u32[]{:S(2)}) copy-start(bf16[2,256,2048]{2,1,0:T(8,128)(2,1)} %get-tuple-element.19) | copy-start | bytes 6291460

commit v2 on v1

--- a/solution.py
+++ b/solution.py
@@ -33,11 +33,11 @@
 def kernel(
     ep, tp, cap,
     tok_ref, cot_ref, gid_ref, wid_ref, gw_ref, wg_ref, wu_ref, wd_ref,
-    dtok_ref, dgate_ref, gwg_ref, gwu_ref, gwd_ref,
+    place_ref, back, gate_back, vwg, vwu, vwd,
     src, placed, rows_in, wg, wu, wd, acc, gate_b, up_b, act_c,
-    to_partner, from_partner, dx_acc, to_x, from_x, to_ep, back,
-    gate_in, gate_sum, gate_back, vwg, vwu, vwd,
-    load_sem, out_sem, own_sem, send1, recv_rows, send_x, send_p, send_p2,
+    to_partner, from_partner, dx_acc, to_x, from_x, to_ep,
+    gate_in, gate_sum,
+    load_sem, own_sem, send1, recv_rows, send_x, send_p, send_p2,
     dxp_send, dxp_recv, dxx_send, dxx_recv, dxe_send, dxe_recv,
     gt_send, gt_recv, ge_send, ge_recv,
 ):
@@ -71,24 +71,30 @@
         load.start()
 
     group = gid_ref[...]
-    in_group = (group == lax.broadcasted_iota(jnp.int32, (tok_rows, LANES), 1)).astype(jnp.float32)
+    groups = -(-ep // 16) * 16
+    in_group = (
+        lax.broadcasted_iota(jnp.int32, (groups, tok_rows), 0) == group
+    ).astype(jnp.float32)
     earlier = (
         lax.broadcasted_iota(jnp.int32, (tok_rows, tok_rows), 0)
-        > lax.broadcasted_iota(jnp.int32, (tok_rows, tok_rows), 1)
+        < lax.broadcasted_iota(jnp.int32, (tok_rows, tok_rows), 1)
     ).astype(jnp.float32).astype(bf16)
-    before = dot(earlier, in_group.astype(bf16))
-    rank = jnp.sum(before * in_group, axis=1, keepdims=True).astype(jnp.int32)
-    slot_lane = lax.broadcasted_iota(jnp.int32, (tok_rows, slots), 1)
-    place = (slot_lane == group * cap + rank).astype(jnp.float32).astype(bf16)
-    lane = lax.broadcasted_iota(jnp.int32, (tok_rows, LANES), 1)
+    before = dot(in_group.astype(bf16), earlier)
+    rank = jnp.sum(before * in_group, axis=0, keepdims=True).astype(jnp.int32)
+    slot_row = lax.broadcasted_iota(jnp.int32, (slots, tok_rows), 0)
+    place = (slot_row == group * cap + rank).astype(jnp.float32).astype(bf16)
+    place_ref[0] = place
+    place_ref[1] = (slot_row == e_me * cap + rank).astype(jnp.float32).astype(bf16)
+    lane_row = lax.broadcasted_iota(jnp.int32, (LANES, tok_rows), 0)
     weights = gw_ref[...].astype(jnp.float32)
-    comb = jnp.zeros((tok_rows, LANES), jnp.float32)
-    for k in range(weights.shape[1]):
-        comb = comb + jnp.where(lane == wid_ref[:, k : k + 1], weights[:, k : k + 1], 0.0)
-    src[:, pl.ds(2 * cs, LANES)] = comb.astype(bf16)
+    comb = jnp.zeros((LANES, tok_rows), jnp.float32)
+    for k in range(weights.shape[0]):
+        comb = comb + jnp.where(lane_row == wid_ref[k : k + 1, :], weights[k : k + 1, :], 0.0)
+    placed[:, pl.ds(2 * cs, LANES)] = dot(place, comb.astype(bf16), NT).astype(bf16)
     loads[0].wait()
+    placed[:, pl.ds(0, cs)] = dot(place, src[:, pl.ds(0, cs)]).astype(bf16)
     loads[1].wait()
-    placed[...] = dot(place, src[...], TN).astype(bf16)
+    placed[:, pl.ds(cs, cs)] = dot(place, src[:, pl.ds(cs, cs)]).astype(bf16)
 
     pl.semaphore_wait(barrier, ep + tp - 2)
 
@@ -288,14 +294,6 @@
     gate_back[e_me] = total
     each(ep - 1, lambda i: gate_ep(i + 1).start())
 
-    def outs(q):
-        cols = share(q)
-        return [
-            pltpu.make_async_copy(vwg.at[:, cols, :], gwg_ref.at[:, cols, :], out_sem.at[q, 0]),
-            pltpu.make_async_copy(vwu.at[:, cols, :], gwu_ref.at[:, cols, :], out_sem.at[q, 1]),
-            pltpu.make_async_copy(vwd.at[:, :, cols], gwd_ref.at[:, :, cols], out_sem.at[q, 2]),
-        ]
-
     def weight_grads(q):
         x_t = rows_in[q, :, pl.ds(0, cs)].T
         yq = rows_in[q, :, pl.ds(cs, cs)]
@@ -303,8 +301,6 @@
             vwg[e, share(q), :] = dot(x_t, gate_b[e]).astype(bf16)
             vwu[e, share(q), :] = dot(x_t, up_b[e]).astype(bf16)
             vwd[e, :, share(q)] = dot(act_c[e], yq, TN).astype(bf16)
-        for copy in outs(q):
-            copy.start()
 
     def dx_ep(d):
         g = lax.rem(e_me + d, ep)
@@ -346,16 +342,6 @@
             send_sem=ge_send.at[0], recv_sem=ge_recv.at[g],
             device_id=(g, t_me), device_id_type=MESH).wait_recv()
     each(ep - 1, gate_arrived)
-    pick = (slot_lane == e_me * cap + rank).astype(jnp.float32).astype(bf16)
-    sums = gate_back[...].reshape(ep * 8, slots)
-    high = sums.astype(bf16)
-    low = (sums - high.astype(jnp.float32)).astype(bf16)
-    dense = dot(pick, high, NT) + dot(pick, low, NT)
-    row_lane = lax.broadcasted_iota(jnp.int32, (tok_rows, ep * 8), 1)
-    for k in range(weights.shape[1]):
-        wanted = row_lane == group * 8 + wid_ref[:, k : k + 1]
-        dgate_ref[:, k : k + 1] = jnp.sum(jnp.where(wanted, dense, 0.0), axis=1, keepdims=True)
-
     def back_arrived(i):
         g = lax.rem(e_me + 1 + i, ep)
         pltpu.make_async_remote_copy(
@@ -363,7 +349,6 @@
             send_sem=dxe_send.at[0], recv_sem=dxe_recv.at[g],
             device_id=(g, t_me), device_id_type=MESH).wait_recv()
     each(ep - 1, back_arrived)
-    dtok_ref[...] = dot(place, back[...]).astype(bf16)
 
     def sent1(i):
         d = i + 1
@@ -383,10 +368,30 @@
     each(nx, lambda k: dx_partner(k).wait_send())
     each(tp - 1, lambda i: gate_tp(i).wait_send())
 
-    def written(q):
-        for copy in outs(q):
-            copy.wait()
-    each(tp, written)
+
+def finish(
+    place_ref, back, gate_back, vwg, vwu, vwd, gid_ref, wid_ref,
+    dtok_ref, dgate_ref, gwg_ref, gwu_ref, gwd_ref, sem,
+):
+    copies = [
+        pltpu.make_async_copy(a, b, sem.at[i])
+        for i, (a, b) in enumerate(((vwg, gwg_ref), (vwu, gwu_ref), (vwd, gwd_ref)))
+    ]
+    for copy in copies:
+        copy.start()
+    ep, _, slots = gate_back.shape
+    tok_rows = place_ref.shape[2]
+    dtok_ref[...] = dot(place_ref[0], back[...], TN).astype(jnp.bfloat16)
+    sums = gate_back[...].reshape(ep * 8, slots)
+    high = sums.astype(jnp.bfloat16)
+    low = (sums - high.astype(jnp.float32)).astype(jnp.bfloat16)
+    dense = dot(high, place_ref[1]) + dot(low, place_ref[1])
+    row = lax.broadcasted_iota(jnp.int32, (ep * 8, tok_rows), 0)
+    for k in range(wid_ref.shape[0]):
+        wanted = row == gid_ref[...] * 8 + wid_ref[k : k + 1, :]
+        dgate_ref[k : k + 1, :] = jnp.sum(jnp.where(wanted, dense, 0.0), axis=0, keepdims=True)
+    for copy in copies:
+        copy.wait()
 
 
 def on_device(tokens, cotangent, group_ids, within_ids, gate_weights, w_gate, w_up, w_down):
@@ -401,10 +406,10 @@
     nx = tp // 2
     bf16, f32 = jnp.bfloat16, jnp.float32
     dma = pltpu.SemaphoreType.DMA
-    anywhere = pl.BlockSpec(memory_space=pl.ANY)
+    hbm = pl.BlockSpec(memory_space=pltpu.HBM)
     vmem = pl.BlockSpec(memory_space=pltpu.VMEM)
     scratch = [
-        pltpu.VMEM((tok_rows, 2 * cs + LANES), bf16),
+        pltpu.VMEM((tok_rows, 2 * cs), bf16),
         pltpu.VMEM((slots, 2 * cs + LANES), bf16),
         pltpu.VMEM((tp, slots, 2 * cs + LANES), bf16),
         pltpu.VMEM(w_gate.shape, bf16),
@@ -420,33 +425,45 @@
         pltpu.VMEM((nx - 1, slots, cs), bf16),
         pltpu.VMEM((nx - 1, slots, cs), bf16),
         pltpu.VMEM((slots, cs), bf16),
-        pltpu.VMEM((slots, cs), bf16),
         pltpu.VMEM((tp, 8, slots), f32),
         pltpu.VMEM((8, slots), f32),
-        pltpu.VMEM((ep, 8, slots), f32),
-        pltpu.VMEM(w_gate.shape, bf16),
-        pltpu.VMEM(w_up.shape, bf16),
-        pltpu.VMEM(w_down.shape, bf16),
-        dma((5,)), dma((tp, 3)), dma((1,)), dma((ep,)), dma((tp, ep)),
+        dma((5,)), dma((1,)), dma((ep,)), dma((tp, ep)),
         dma((nx - 1, ep)), dma((ep,)), dma((nx - 1, ep)),
         dma((nx,)), dma((nx,)), dma((nx - 1, ep)), dma((nx - 1, ep)), dma((ep,)), dma((ep,)),
         dma((tp,)), dma((tp,)), dma((ep,)), dma((ep,)),
     ]
-    return pl.pallas_call(
+    gid, wid, gw = group_ids.T, within_ids.T, gate_weights.T
+    kept = pl.pallas_call(
         functools.partial(kernel, ep, tp, cap),
         out_shape=(
+            pltpu.VMEM((2, slots, tok_rows), bf16),
+            pltpu.VMEM((slots, cs), bf16),
+            pltpu.VMEM((ep, 8, slots), f32),
+            pltpu.VMEM(w_gate.shape, bf16),
+            pltpu.VMEM(w_up.shape, bf16),
+            pltpu.VMEM(w_down.shape, bf16),
+        ),
+        in_specs=[hbm, hbm, vmem, vmem, vmem, hbm, hbm, hbm],
+        out_specs=(vmem,) * 6,
+        scratch_shapes=scratch,
+        compiler_params=pltpu.CompilerParams(
+            collective_id=0, has_side_effects=True, vmem_limit_bytes=40 * 1024 * 1024),
+    )(tokens, cotangent, gid, wid, gw, w_gate, w_up, w_down)
+    dtok, dgate, gwg, gwu, gwd = pl.pallas_call(
+        finish,
+        out_shape=(
             jax.ShapeDtypeStruct((tok_rows, cs), bf16),
-            jax.ShapeDtypeStruct(within_ids.shape, f32),
+            jax.ShapeDtypeStruct(wid.shape, f32),
             jax.ShapeDtypeStruct(w_gate.shape, bf16),
             jax.ShapeDtypeStruct(w_up.shape, bf16),
             jax.ShapeDtypeStruct(w_down.shape, bf16),
         ),
-        in_specs=[anywhere, anywhere, vmem, vmem, vmem, anywhere, anywhere, anywhere],
-        out_specs=(vmem, vmem, anywhere, anywhere, anywhere),
-        scratch_shapes=scratch,
-        compiler_params=pltpu.CompilerParams(
-            collective_id=0, has_side_effects=True, vmem_limit_bytes=56 * 1024 * 1024),
-    )(tokens, cotangent, group_ids, within_ids, gate_weights, w_gate, w_up, w_down)
+        in_specs=[vmem] * 8,
+        out_specs=(vmem, vmem, hbm, hbm, hbm),
+        scratch_shapes=[dma((3,))],
+        compiler_params=pltpu.CompilerParams(vmem_limit_bytes=12 * 1024 * 1024),
+    )(*kept, gid, wid)
+    return dtok, dgate.T, gwg, gwu, gwd
 
 
 def solution(mesh):

time: 58.9 us -> 55.1 us (0.935)
  local copies, waits for them, and re-layouts: 14.3 us -> 9 us
  Pallas kernels: 43.7 us -> 45.1 us
    unnamed x11 -> x16, local copies, waits for them, and re-layouts: 12.7 us -> 9 us
    pallas_call x1 -> x0, local copies, waits for them, and re-layouts: 1.55 us -> none  [on_device(): pl.pallas_call(functools.partial(kernel, ep, tp, cap), out_shape=(jax.Sha...]
    pallas_call x1 -> x2, Pallas kernels: 43.7 us -> 45.1 us  [the longest x1 41.6 us: on_device(): pl.pallas_call(functools.partial(kernel, ep, tp, cap), out_shape=(pltpu.V...]
where the time goes in v2:
time: 55.1 us; the launch traced here: 54.7 us
  Pallas kernels  45.1 us (82%)
  local copies, waits for them, and re-layouts  9 us (16%)
  between operations  0.66 us (1%)
    pallas_call x1, Pallas kernels, on_device(): pl.pallas_call(functools.partial(kernel, ep, tp, cap), out_shape=(pltpu.V...  41.6 us
    unnamed x16, local copies, waits for them, and re-layouts  9 us
    pallas_call x1, Pallas kernels, on_device(): pl.pallas_call(finish, out_shape=(jax.ShapeDtypeStruct((tok_rows, cs), bf...  3.44 us

profile of v2, /device:TPU:0, one launch (start us, length us, event | category | flops | bytes accessed | tf_op | source)
XLA Modules:
  0.0 54.7 jit_solution(8908876309824560783)
XLA Ops:
  0.6 0.0 copy-start
  0.6 1.6 %copy-done = bf16[2,2048,256]{2,1,0:T(8,128)(2,1)S(1)} copy-done((bf16[2,2048,256]{2,1,0:T(8,128)(2,1)S(1)}, bf16[2,2048,256]{2,1,0:T(8,128)(2,1)}, u32[]{:S(2)}) %copy-start) | copy-done | bytes 2097176
  2.2 0.0 copy-start.1
  2.2 1.6 %copy-done.1 = bf16[2,2048,256]{2,1,0:T(8,128)(2,1)S(1)} copy-done((bf16[2,2048,256]{2,1,0:T(8,128)(2,1)S(1)}, bf16[2,2048,256]{2,1,0:T(8,128)(2,1)}, u32[]{:S(2)}) %copy-start.1) | copy-done | bytes 2097176
  3.8 0.0 copy-start.2
  3.8 1.6 %copy-done.2 = bf16[2,256,2048]{2,1,0:T(8,128)(2,1)S(1)} copy-done((bf16[2,256,2048]{2,1,0:T(8,128)(2,1)S(1)}, bf16[2,256,2048]{2,1,0:T(8,128)(2,1)}, u32[]{:S(2)}) %copy-start.2) | copy-done | bytes 2097176
  5.4 0.0 copy-start.3
  5.4 1.1 %copy-done.3 = bf16[168,2048]{1,0:T(8,128)(2,1)S(1)} copy-done((bf16[168,2048]{1,0:T(8,128)(2,1)S(1)}, bf16[168,2048]{1,0:T(8,128)(2,1)}, u32[]{:S(2)}) %copy-start.3) | copy-done | bytes 688152
  6.5 0.0 copy-start.4
  6.5 1.1 %copy-done.4 = bf16[168,2048]{1,0:T(8,128)(2,1)S(1)} copy-done((bf16[168,2048]{1,0:T(8,128)(2,1)S(1)}, bf16[168,2048]{1,0:T(8,128)(2,1)}, u32[]{:S(2)}) %copy-start.4) | copy-done | bytes 688152
  7.6 0.0 copy-start.5
  7.6 0.7 %copy-done.5 = s32[168,2]{0,1:T(2,128)S(1)} copy-done((s32[168,2]{0,1:T(2,128)S(1)}, s32[168,2]{0,1:T(2,128)}, u32[]{:S(2)}) %copy-start.5) | copy-done | bytes 1368
  8.3 0.0 copy-start.6
  8.3 0.7 %copy-done.6 = s32[168,1]{0,1:T(1,128)S(1)} copy-done((s32[168,1]{0,1:T(1,128)S(1)}, s32[168,1]{0,1:T(1,128)}, u32[]{:S(2)}) %copy-start.6) | copy-done | bytes 696
  9.0 0.0 copy-start.7
  9.0 0.7 %copy-done.7 = bf16[168,2]{0,1:T(2,128)(2,1)S(1)} copy-done((bf16[168,2]{0,1:T(2,128)(2,1)S(1)}, bf16[168,2]{0,1:T(2,128)(2,1)}, u32[]{:S(2)}) %copy-start.7) | copy-done | bytes 696
  9.6 41.6 %shard_map.119 = (bf16[2,256,168]{2,1,0:T(8,128)(2,1)S(1)}, bf16[256,512]{1,0:T(8,128)(2,1)S(1)}, f32[8,8,256]{2,1,0:T(8,128)S(1)}, bf16[2,2048,256]{2,1,0:T(8,1...) custom-call(bf16[168,2048]{1,0:T(8,128)(2,1)S(1)} %copy-done.3, ...), custom_call_target="tpu_custom_call" | custom-call | tf_op jit(solution)/shard_map/pallas_call | solution.py:436
  51.3 3.4 %shard_map.120 = (bf16[168,512]{1,0:T(8,128)(2,1)}, f32[2,168]{1,0:T(2,128)}, bf16[2,2048,256]{2,1,0:T(8,128)(2,1)}, bf16[2,2048,256]{2,1,0:T(8,128)(2,1)}, bf16[2,256,2048]{2,1,0:T(8,128)(2,1)}) custom-call(bf16[2,256,168]{2,1,0:T(8,128)(2,1)S(1)} %get-tuple-element.16.place_ref, bf16[256,512]{1,0:T(8,128)(2,1)S(1)} %get-tuple-element.17.back, ...), custom_call_target="tpu_custom_call" | custom-call | tf_op jit(solution)/shard_map/pallas_call | solution.py:452
Async XLA Ops:
  0.6 1.6 %copy-start = (bf16[2,2048,256]{2,1,0:T(8,128)(2,1)S(1)}, bf16[2,2048,256]{2,1,0:T(8,128)(2,1)}, u32[]{:S(2)}) copy-start(bf16[2,2048,256]{2,1,0:T(8,128)(2,1)} %wg_ref.1) | copy-start | bytes 6291460
  2.2 1.6 %copy-start.1 = (bf16[2,2048,256]{2,1,0:T(8,128)(2,1)S(1)}, bf16[2,2048,256]{2,1,0:T(8,128)(2,1)}, u32[]{:S(2)}) copy-start(bf16[2,2048,256]{2,1,0:T(8,128)(2,1)} %wu_ref.1) | copy-start | bytes 6291460
  3.8 1.6 %copy-start.2 = (bf16[2,256,2048]{2,1,0:T(8,128)(2,1)S(1)}, bf16[2,256,2048]{2,1,0:T(8,128)(2,1)}, u32[]{:S(2)}) copy-start(bf16[2,256,2048]{2,1,0:T(8,128)(2,1)} %wd_ref.1) | copy-start | bytes 6291460
  5.4 1.1 %copy-start.3 = (bf16[168,2048]{1,0:T(8,128)(2,1)S(1)}, bf16[168,2048]{1,0:T(8,128)(2,1)}, u32[]{:S(2)}) copy-start(bf16[168,2048]{1,0:T(8,128)(2,1)} %tok_ref.1) | copy-start | bytes 2064388
  6.5 1.1 %copy-start.4 = (bf16[168,2048]{1,0:T(8,128)(2,1)S(1)}, bf16[168,2048]{1,0:T(8,128)(2,1)}, u32[]{:S(2)}) copy-start(bf16[168,2048]{1,0:T(8,128)(2,1)} %cot_ref.1) | copy-start | bytes 2064388
  7.6 0.7 %copy-start.5 = (s32[168,2]{0,1:T(2,128)S(1)}, s32[168,2]{0,1:T(2,128)}, u32[]{:S(2)}) copy-start(s32[168,2]{0,1:T(2,128)} %param.11) | copy-start | bytes 4036
  8.3 0.7 %copy-start.6 = (s32[168,1]{0,1:T(1,128)S(1)}, s32[168,1]{0,1:T(1,128)}, u32[]{:S(2)}) copy-start(s32[168,1]{0,1:T(1,128)} %param.10) | copy-start | bytes 2020
  9.0 0.7 %copy-start.7 = (bf16[168,2]{0,1:T(2,128)(2,1)S(1)}, bf16[168,2]{0,1:T(2,128)(2,1)}, u32[]{:S(2)}) copy-start(bf16[168,2]{0,1:T(2,128)(2,1)} %param.12) | copy-start | bytes 2020

commit v3 on v2

--- a/solution.py
+++ b/solution.py
@@ -47,6 +47,7 @@
     x_me = lax.div(t_me, 2)
     partner = t_me + 1 - 2 * core
     nx = tp // 2
+    gate_lanes = gate_back.shape[2]
     tok_rows, width = tok_ref.shape
     cs = width // tp
     slots = ep * cap
@@ -67,7 +68,7 @@
         pltpu.make_async_copy(wu_ref, wu, load_sem.at[3]),
         pltpu.make_async_copy(wd_ref, wd, load_sem.at[4]),
     ]
-    for load in loads:
+    for load in loads[:2]:
         load.start()
 
     group = gid_ref[...]
@@ -84,7 +85,7 @@
     slot_row = lax.broadcasted_iota(jnp.int32, (slots, tok_rows), 0)
     place = (slot_row == group * cap + rank).astype(jnp.float32).astype(bf16)
     place_ref[0] = place
-    place_ref[1] = (slot_row == e_me * cap + rank).astype(jnp.float32).astype(bf16)
+    place_ref[1] = (slot_row == e_me * cap % gate_lanes + rank).astype(jnp.float32).astype(bf16)
     lane_row = lax.broadcasted_iota(jnp.int32, (LANES, tok_rows), 0)
     weights = gw_ref[...].astype(jnp.float32)
     comb = jnp.zeros((LANES, tok_rows), jnp.float32)
@@ -94,21 +95,31 @@
     loads[0].wait()
     placed[:, pl.ds(0, cs)] = dot(place, src[:, pl.ds(0, cs)]).astype(bf16)
     loads[1].wait()
+    for load in loads[2:]:
+        load.start()
     placed[:, pl.ds(cs, cs)] = dot(place, src[:, pl.ds(cs, cs)]).astype(bf16)
 
     pl.semaphore_wait(barrier, ep + tp - 2)
+
+    def xor(d):
+        value, bit = 0, 1
+        while bit < ep:
+            value = value + (e_me // bit + d // bit) % 2 * bit
+            bit *= 2
+        return value
+
+    def target(d):
+        return xor(d) if ep & (ep - 1) == 0 else lax.rem(e_me + d, ep)
+
+    def source(d):
+        return xor(d) if ep & (ep - 1) == 0 else lax.rem(e_me - d + ep, ep)
 
     def block(e):
         return pl.ds(aligned(e * cap, 16), cap)
 
     distances = list(range(ep))
-    if ep <= 8:
-        distances = [0]
-        for k in range(1, ep // 2 + 1):
-            distances += sorted({k, ep - k})
-
     def stage1(d):
-        g = lax.rem(e_me + d, ep)
+        g = target(d)
         return pltpu.make_async_remote_copy(
             src_ref=placed.at[block(g)], dst_ref=rows_in.at[t_me, block(e_me)],
             send_sem=send1.at[d], recv_sem=recv_rows.at[t_me, e_me],
@@ -139,7 +150,7 @@
         return lax.rem(x_me + k, nx) * 2 + core
 
     def to_peers(d):
-        e = lax.rem(e_me - d + ep, ep)
+        e = source(d)
         copies = [forward(t_me, e, send_x.at[k - 1, d], x_peer(k)) for k in range(1, nx)]
         return copies + [forward(t_me, e, send_p.at[d], partner)]
 
@@ -148,7 +159,7 @@
             copy.start()
 
     def relays(d):
-        e = lax.rem(e_me - d + ep, ep)
+        e = source(d)
         return [(x_peer(k), e, forward(x_peer(k), e, send_p2.at[k - 1, d], partner))
                 for k in range(1, nx)]
 
@@ -161,15 +172,13 @@
     stage2(0)
     if ep <= 8:
         for i, d in enumerate(distances[1:]):
-            arrived(t_me, lax.rem(e_me - d + ep, ep), 2 * cs + LANES)
+            arrived(t_me, source(d), 2 * cs + LANES)
             stage2(d)
-            stage3(distances[i])
     else:
         def later(i):
-            arrived(t_me, lax.rem(e_me - i - 1 + ep, ep), 2 * cs + LANES)
+            arrived(t_me, source(i + 1), 2 * cs + LANES)
             stage2(i + 1)
         each(ep - 1, later)
-        each(ep - 1, stage3)
 
     for load in loads[2:]:
         load.wait()
@@ -192,7 +201,11 @@
         each(ep, lambda e: arrived(q, e, 2 * cs))
 
     hidden(t_me, True)
-    stage3(distances[-1])
+    if ep <= 8:
+        for d in distances:
+            stage3(d)
+    else:
+        each(ep, stage3)
     all_arrived(partner)
     hidden(partner, False)
 
@@ -245,11 +258,9 @@
         k = nx - 1 - i
         to_partner[k] = dx_of(lax.rem(x_me + k, nx) * 2 + 1 - core).astype(bf16)
         dx_partner(k).start()
-    each(nx, give_partner)
-    each(tp - 1, lambda i: gate_tp(i).start())
 
     def dx_x(k, d):
-        e = lax.rem(e_me + d, ep)
+        e = target(d)
         return pltpu.make_async_remote_copy(
             src_ref=to_x.at[k - 1, block(e)], dst_ref=from_x.at[k - 1, block(e)],
             send_sem=dxx_send.at[k - 1, d], recv_sem=dxx_recv.at[k - 1, d],
@@ -269,16 +280,25 @@
         dx_partner(k).wait_recv()
         to_x[k - 1] = (mine + from_partner[k].astype(jnp.float32)).astype(bf16)
         walk(lambda i, d: dx_x(k, d).start())
-    each(nx - 1, lambda i: give_x(i + 1))
+    each(tp - 1, lambda i: gate_tp(i).start())
+
+    def cross(i):
+        give_partner(i)
+        give_x(nx - 1 - i)
+    each(nx - 1, cross)
+    give_partner(nx - 1)
     mine = dx_of(t_me)
     dx_partner(0).wait_recv()
     dx_acc[...] = mine + from_partner[0].astype(jnp.float32)
 
+    def gate_tile(e):
+        return pl.ds(pl.multiple_of(e * cap // gate_lanes * gate_lanes, LANES), gate_lanes)
+
     def gate_ep(d):
         return pltpu.make_async_remote_copy(
-            src_ref=gate_sum, dst_ref=gate_back.at[e_me],
+            src_ref=gate_sum.at[:, gate_tile(target(d))], dst_ref=gate_back.at[e_me],
             send_sem=ge_send.at[d], recv_sem=ge_recv.at[e_me],
-            device_id=(lax.rem(e_me + d, ep), t_me), device_id_type=MESH)
+            device_id=(target(d), t_me), device_id_type=MESH)
 
     def gate_wait(i):
         q = lax.rem(t_me + 1 + i, tp)
@@ -286,13 +306,15 @@
             src_ref=gate_in.at[q], dst_ref=gate_in.at[q],
             send_sem=gt_send.at[i], recv_sem=gt_recv.at[q],
             device_id=(e_me, q), device_id_type=MESH).wait_recv()
-    each(tp - 1, gate_wait)
-    total = gate_in[0]
-    for q in range(1, tp):
-        total = total + gate_in[q]
-    gate_sum[...] = total
-    gate_back[e_me] = total
-    each(ep - 1, lambda i: gate_ep(i + 1).start())
+
+    def gates_on():
+        each(tp - 1, gate_wait)
+        total = gate_in[0]
+        for q in range(1, tp):
+            total = total + gate_in[q]
+        gate_sum[...] = total
+        gate_back[e_me] = gate_sum[:, gate_tile(e_me)]
+        each(ep - 1, lambda i: gate_ep(i + 1).start())
 
     def weight_grads(q):
         x_t = rows_in[q, :, pl.ds(0, cs)].T
@@ -303,14 +325,14 @@
             vwd[e, :, share(q)] = dot(act_c[e], yq, TN).astype(bf16)
 
     def dx_ep(d):
-        g = lax.rem(e_me + d, ep)
+        g = target(d)
         return pltpu.make_async_remote_copy(
             src_ref=to_ep.at[block(g)], dst_ref=back.at[block(e_me)],
             send_sem=dxe_send.at[d], recv_sem=dxe_recv.at[e_me],
             device_id=(g, t_me), device_id_type=MESH)
 
     def finish_chunk(d):
-        rows = block(lax.rem(e_me + d, ep))
+        rows = block(target(d))
         value = dx_acc[rows, :]
         for k in range(1, nx):
             dx_x(k, d).wait_recv()
@@ -318,7 +340,7 @@
         return value.astype(bf16)
 
     def chunk(i, d):
-        to_ep[block(lax.rem(e_me + d, ep)), :] = finish_chunk(d)
+        to_ep[block(target(d)), :] = finish_chunk(d)
         dx_ep(d).start()
 
     if ep <= 8:
@@ -328,17 +350,20 @@
             if i % 2 == 0 and done < tp:
                 weight_grads(done)
                 done += 1
+            if i == min(2, ep - 2):
+                gates_on()
         for q in range(done, tp):
             weight_grads(q)
     else:
         each(ep - 1, lambda i: chunk(i, ep - 1 - i))
         each(tp, weight_grads)
+        gates_on()
     back[block(e_me), :] = finish_chunk(0)
 
     def gate_arrived(i):
         g = lax.rem(e_me + 1 + i, ep)
         pltpu.make_async_remote_copy(
-            src_ref=gate_sum, dst_ref=gate_back.at[g],
+            src_ref=gate_sum.at[:, gate_tile(g)], dst_ref=gate_back.at[g],
             send_sem=ge_send.at[0], recv_sem=ge_recv.at[g],
             device_id=(g, t_me), device_id_type=MESH).wait_recv()
     each(ep - 1, gate_arrived)
@@ -371,25 +396,34 @@
 
 def finish(
     place_ref, back, gate_back, vwg, vwu, vwd, gid_ref, wid_ref,
-    dtok_ref, dgate_ref, gwg_ref, gwu_ref, gwd_ref, sem,
+    dtok_ref, dgate_ref, gwg_ref, gwu_ref, gwd_ref, dtok, dgate, sem,
 ):
-    copies = [
-        pltpu.make_async_copy(a, b, sem.at[i])
-        for i, (a, b) in enumerate(((vwg, gwg_ref), (vwu, gwu_ref), (vwd, gwd_ref)))
-    ]
+    copies = []
+    for a, b in ((vwg, gwg_ref), (vwu, gwu_ref), (vwd, gwd_ref)):
+        experts, rows, _ = a.shape
+        for e in range(experts):
+            for half in range(2):
+                part = pl.ds(half * (rows // 2), rows // 2)
+                copies.append(pltpu.make_async_copy(
+                    a.at[e, part], b.at[e, part], sem.at[2 + len(copies)]))
     for copy in copies:
         copy.start()
     ep, _, slots = gate_back.shape
     tok_rows = place_ref.shape[2]
-    dtok_ref[...] = dot(place_ref[0], back[...], TN).astype(jnp.bfloat16)
+    dtok[...] = dot(place_ref[0], back[...], TN).astype(jnp.bfloat16)
+    copies.append(pltpu.make_async_copy(dtok, dtok_ref, sem.at[0]))
+    copies[-1].start()
     sums = gate_back[...].reshape(ep * 8, slots)
     high = sums.astype(jnp.bfloat16)
     low = (sums - high.astype(jnp.float32)).astype(jnp.bfloat16)
-    dense = dot(high, place_ref[1]) + dot(low, place_ref[1])
+    pick = place_ref[1, :slots, :]
+    dense = dot(high, pick) + dot(low, pick)
     row = lax.broadcasted_iota(jnp.int32, (ep * 8, tok_rows), 0)
     for k in range(wid_ref.shape[0]):
         wanted = row == gid_ref[...] * 8 + wid_ref[k : k + 1, :]
-        dgate_ref[k : k + 1, :] = jnp.sum(jnp.where(wanted, dense, 0.0), axis=0, keepdims=True)
+        dgate[k : k + 1, :] = jnp.sum(jnp.where(wanted, dense, 0.0), axis=0, keepdims=True)
+    copies.append(pltpu.make_async_copy(dgate, dgate_ref, sem.at[1]))
+    copies[-1].start()
     for copy in copies:
         copy.wait()
 
@@ -402,6 +436,7 @@
     cap = (3 * tok_rows + 2 * ep - 1) // (2 * ep)
     cap = -(-cap // 16) * 16
     slots = ep * cap
+    gate_lanes = LANES if LANES % cap == 0 and slots % LANES == 0 else slots
     cs = width // tp
     nx = tp // 2
     bf16, f32 = jnp.bfloat16, jnp.float32
@@ -438,7 +473,7 @@
         out_shape=(
             pltpu.VMEM((2, slots, tok_rows), bf16),
             pltpu.VMEM((slots, cs), bf16),
-            pltpu.VMEM((ep, 8, slots), f32),
+            pltpu.VMEM((ep, 8, gate_lanes), f32),
             pltpu.VMEM(w_gate.shape, bf16),
             pltpu.VMEM(w_up.shape, bf16),
             pltpu.VMEM(w_down.shape, bf16),
@@ -447,7 +482,7 @@
         out_specs=(vmem,) * 6,
         scratch_shapes=scratch,
         compiler_params=pltpu.CompilerParams(
-            collective_id=0, has_side_effects=True, vmem_limit_bytes=40 * 1024 * 1024),
+            collective_id=0, has_side_effects=True, vmem_limit_bytes=57 * 1024 * 1024),
     )(tokens, cotangent, gid, wid, gw, w_gate, w_up, w_down)
     dtok, dgate, gwg, gwu, gwd = pl.pallas_call(
         finish,
@@ -459,8 +494,12 @@
             jax.ShapeDtypeStruct(w_down.shape, bf16),
         ),
         in_specs=[vmem] * 8,
-        out_specs=(vmem, vmem, hbm, hbm, hbm),
-        scratch_shapes=[dma((3,))],
+        out_specs=(hbm,) * 5,
+        scratch_shapes=[
+            pltpu.VMEM((tok_rows, cs), bf16),
+            pltpu.VMEM(wid.shape, f32),
+            dma((2 + 6 * experts,)),
+        ],
         compiler_params=pltpu.CompilerParams(vmem_limit_bytes=12 * 1024 * 1024),
     )(*kept, gid, wid)
     return dtok, dgate.T, gwg, gwu, gwd

time: 55.1 us -> 44.1 us (0.80)
  local copies, waits for them, and re-layouts: 9 us -> 0.01 us
  Pallas kernels: 45.1 us -> 43.3 us
    unnamed x16 -> x4, local copies, waits for them, and re-layouts: 9 us -> 0.01 us
    pallas_call x1, Pallas kernels: 41.6 us -> 40.5 us  [on_device(): pl.pallas_call(functools.partial(kernel, ep, tp, cap), out_shape=(pltpu.V...]
    pallas_call x1, Pallas kernels: 3.44 us -> 2.82 us  [on_device(): pl.pallas_call(finish, out_shape=(jax.ShapeDtypeStruct((tok_rows, cs), bf...]
where the time goes in v3:
time: 44.1 us; the launch traced here: 44 us
  Pallas kernels  43.3 us (98%)
  between operations  0.67 us (2%)
    pallas_call x1, Pallas kernels, on_device(): pl.pallas_call(functools.partial(kernel, ep, tp, cap), out_shape=(pltpu.V...  40.5 us
    pallas_call x1, Pallas kernels, on_device(): pl.pallas_call(finish, out_shape=(jax.ShapeDtypeStruct((tok_rows, cs), bf...  2.82 us

profile of v3, /device:TPU:0, one launch (start us, length us, event | category | flops | bytes accessed | tf_op | source)
XLA Modules:
  0.0 44.0 jit_solution(17925269628753032345)
XLA Ops:
  0.6 0.0 copy-start
  0.6 0.0 copy-start.1
  0.7 40.5 %shard_map.119 = (bf16[2,256,168]{2,1,0:T(8,128)(2,1)S(1)}, bf16[256,512]{1,0:T(8,128)(2,1)S(1)}, f32[8,8,128]{2,1,0:T(8,128)S(1)}, bf16[2,2048,256]{2,1,0:T(8,1...) custom-call(bf16[168,2048]{1,0:T(8,128)(2,1)} %tok_ref.1, bf16[168,2048]{1,0:T(8,128)(2,1)} %cot_ref.1, ...), custom_call_target="tpu_custom_call" | custom-call | tf_op jit(solution)/shard_map/pallas_call | solution.py:471
  41.1 0.0 copy-done
  41.2 0.0 copy-done.1
  41.2 2.8 %shard_map.120 = (bf16[168,512]{1,0:T(8,128)(2,1)}, f32[2,168]{1,0:T(2,128)}, bf16[2,2048,256]{2,1,0:T(8,128)(2,1)}, bf16[2,2048,256]{2,1,0:T(8,128)(2,1)}, bf16[2,256,2048]{2,1,0:T(8,128)(2,1)}) custom-call(bf16[2,256,168]{2,1,0:T(8,128)(2,1)S(1)} %get-tuple-element.16.place_ref, bf16[256,512]{1,0:T(8,128)(2,1)S(1)} %get-tuple-element.17.back, ...), custom_call_target="tpu_custom_call" | custom-call | tf_op jit(solution)/shard_map/pallas_call | solution.py:487
Async XLA Ops:
  0.6 40.5 %copy-start = (s32[168,2]{0,1:T(2,128)S(1)}, s32[168,2]{0,1:T(2,128)}, u32[]{:S(2)}) copy-start(s32[168,2]{0,1:T(2,128)} %param.11) | copy-start | bytes 4036
  0.6 40.5 %copy-start.1 = (s32[168,1]{0,1:T(1,128)S(1)}, s32[168,1]{0,1:T(1,128)}, u32[]{:S(2)}) copy-start(s32[168,1]{0,1:T(1,128)} %param.10) | copy-start | bytes 2020
